TPU v7x, 256 devices: a whole 4x4x8 slice. The times are simulated.
256 devices in a mesh: sp: 32 (over z, y), fs: 4 (over x), tp: 2 (over core).
Axes of the slice: x: 4, y: 4, z: 8, core: 2. Of those that a mesh axis runs over, the one named last changes fastest.
Arguments:
- hidden_in: bfloat16 [4, 8192, 2048], P('fs', 'sp', 'tp'), may hold values from -6 to 6
- sb_query_w: bfloat16 [2048, 1024], P('fs', 'tp'), may hold values from -0.21875 to 0.21875
- sb_key_w: bfloat16 [2048, 1024], P('fs', 'tp'), may hold values from -0.21875 to 0.21875
- sb_value_w: bfloat16 [2048, 1024], P('fs', 'tp'), may hold values from -0.125 to 0.125
- sb_offset: float32 [16], P('tp'), may hold values from -16 to -6
- delta_query_w: bfloat16 [2048, 1024], P('fs', 'tp'), may hold values from -0.125 to 0.125
- delta_key_w: bfloat16 [2048, 1024], P('fs', 'tp'), may hold values from -0.125 to 0.125
- delta_value_w: bfloat16 [2048, 1024], P('fs', 'tp'), may hold values from -0.125 to 0.125
- decay_w: bfloat16 [2048, 8], P(None, 'tp'), may hold values from -0.125 to 0.125
- write_w: bfloat16 [2048, 8], P(None, 'tp'), may hold values from -0.125 to 0.125
- write_bias: float32 [8], P('tp'), may hold values from -7 to 1.5
- decay_log_scale: float32 [8], P('tp'), may hold values from -14 to -3
- decay_shift: float32 [4, 8, 8192], P('fs', 'tp', 'sp'), may hold values from -3 to 0
- head_gain: float32 [128], replicated, may hold values from 0.1 to 1.9
- sb_out_w: bfloat16 [1024, 2048], P('tp'), may hold values from -0.125 to 0.125
- delta_out_w: bfloat16 [1024, 2048], P('tp'), may hold values from -0.125 to 0.125
Outputs:
- mixed_out: bfloat16 [4, 8192, 2048], P('fs', ('sp', 'tp'))
All inputs are finite; a program needn't handle non-finite values.
Results may differ from a plain program's by a relative error of at most 0.015.
Values may be sent and summed in bfloat16 or wider, within the bound.
No kernel may reach another device: no remote copies, remote signals or barrier semaphores. Data moves between devices by JAX's collectives and lax.ppermute only.
A program may use at most 128 MiB of HBM per device.

v0:
```python
import jax
import jax.numpy as jnp
from jax import lax
from jax.sharding import Mesh
from jax.sharding import PartitionSpec as P

SB_DIM = 64
GDN_DIM = 128
BLOCK = 64
SP = ("sp_0", "sp_1")
SP_TP = ("sp_0", "sp_1", "tp")


NORM_EPS = 1e-06


def joined_along(tiles, dim):
    tiles = jnp.moveaxis(tiles, 0, dim)
    shape = tiles.shape
    return tiles.reshape(*shape[:dim], shape[dim] * shape[dim + 1], *shape[dim + 2 :])


def sent_to_all(value, axis):
    devices = lax.axis_size(axis)
    return lax.all_to_all(
        jnp.broadcast_to(value[None], (devices, *value.shape)), axis, 0, 0, tiled=True
    )


def gathered_copies(value, axis, dim):
    return joined_along(sent_to_all(value, axis), dim)


def in_one_piece(arrays, axis, dim, along):
    widths = [a.shape[along] for a in arrays]
    both = jnp.concatenate(arrays, axis=along)
    result = lax.all_gather(both, axis, axis=dim, tiled=True)
    return tuple(jnp.split(result, [sum(widths[:k]) for k in range(1, len(widths))], axis=along))


def neutral_like(value, identity):
    return jax.tree.map(
        lambda part, zero: jnp.zeros_like(part) + jnp.asarray(zero, part.dtype), value, identity
    )


def entering(value, axes, combine, identity):
    before = start = neutral_like(value, identity)
    so_far = value
    for axis in reversed(axes):
        devices, index = (lax.axis_size(axis), lax.axis_index(axis))
        pieces = jax.tree.map(
            lambda part, kind: lax.all_gather(part.astype(kind), axis),
            so_far,
            (jnp.bfloat16, jnp.bfloat16),
        )
        inside, so_far = (start, start)
        for k in range(devices):
            passed = k < index
            so_far = combine(
                so_far, jax.tree.map(lambda part, own: part[k].astype(own.dtype), pieces, value)
            )
            inside = jax.tree.map(lambda new, old: jnp.where(passed, new, old), so_far, inside)
        before = combine(inside, before)
    return before


def split_up(value, dim, devices):
    before, after = (value.shape[:dim], value.shape[dim + 1 :])
    return jnp.moveaxis(value.reshape(*before, devices, -1, *after), dim, 0)


def sent_and_summed(value, axis, dim):
    tiles = split_up(value, dim, lax.axis_size(axis))
    arrived = lax.all_to_all(tiles, axis, split_axis=0, concat_axis=0, tiled=True)
    return arrived.astype(jnp.float32).sum(axis=0)


def unit_lower_inverse(strict_part):
    order_size = strict_part.shape[-1]
    powered = strict_part
    inverse = jnp.eye(order_size, dtype=strict_part.dtype) - strict_part
    for repeat_number in range(max(1, (order_size - 1).bit_length()) - 1):
        powered = jnp.einsum("...ij,...jk->...ik", powered, powered)
        inverse = inverse + jnp.einsum("...ij,...jk->...ik", inverse, powered)
    return inverse


def to_blocks(row_data, block_span):
    blocks_count = row_data.shape[0] // block_span
    shaped = row_data.reshape((blocks_count, block_span) + row_data.shape[1:])
    return jnp.swapaxes(shaped, 1, 2)


def from_blocks(blocked):
    swapped = jnp.swapaxes(blocked, 1, 2)
    return swapped.reshape((-1,) + swapped.shape[2:])


def unit_rows(vectors):
    return vectors * lax.rsqrt(jnp.sum(vectors * vectors, axis=-1, keepdims=True) + NORM_EPS)


def delta_inputs(
    query_proj,
    key_proj,
    value_proj,
    decay_pre,
    write_pre,
    write_bias,
    decay_log_scale,
    shift_rows,
    head_count,
    head_size,
):
    query_act = jax.nn.silu(query_proj.astype(jnp.float32)).reshape(-1, head_count, head_size)
    key_act = jax.nn.silu(key_proj.astype(jnp.float32)).reshape(-1, head_count, head_size)
    value_rows = jax.nn.silu(value_proj.astype(jnp.float32)).reshape(-1, head_count, head_size)
    queries = unit_rows(query_act) * head_size ** (-0.5)
    key_rows = unit_rows(key_act)
    log_decay = -jnp.exp(decay_log_scale) * jax.nn.softplus(decay_pre) + shift_rows
    strength = jax.nn.sigmoid(write_pre + write_bias)
    return (queries, key_rows, value_rows, log_decay, strength)


def delta_prepare(queries, key_rows, value_rows, log_decay, strength):
    block_span = queries.shape[2]
    cumulative = jnp.cumsum(log_decay, axis=-1)
    row_place = lax.broadcasted_iota(jnp.int32, (block_span, block_span), 0)
    col_place = lax.broadcasted_iota(jnp.int32, (block_span, block_span), 1)
    inclusive = col_place <= row_place
    strictly = col_place < row_place
    spread = cumulative[..., :, None] - cumulative[..., None, :]
    decay_table = jnp.where(inclusive, jnp.exp(jnp.where(inclusive, spread, 0.0)), 0.0)
    keys_beta = key_rows * strength[..., None]
    lower_part = jnp.where(
        strictly, jnp.einsum("nhik,nhjk->nhij", keys_beta, key_rows) * decay_table, 0.0
    )
    inverse = unit_lower_inverse(lower_part)
    growth = jnp.exp(cumulative)
    state_updates = jnp.einsum("nhij,nhjv->nhiv", inverse, value_rows * strength[..., None])
    erase_term = jnp.einsum("nhij,nhjk->nhik", inverse, keys_beta * growth[..., None])
    inside_block = jnp.einsum("nhik,nhjk->nhij", queries, key_rows) * decay_table
    boosted_query = queries * growth[..., None]
    damped_keys = key_rows * jnp.exp(cumulative[..., -1:] - cumulative)[..., None]
    decay_per_block = jnp.exp(cumulative[..., -1])
    return (state_updates, erase_term, inside_block, boosted_query, damped_keys, decay_per_block)


def delta_step(memory_state, inputs):
    state_updates, erase_term, inside_block, boosted_query, damped_keys, decay_per_block = inputs
    fixed_values = state_updates - jnp.einsum("mzq,mqc->mzc", erase_term, memory_state)
    produced_rows = jnp.einsum("mzq,mqc->mzc", boosted_query, memory_state) + jnp.einsum(
        "efq,eqn->efn", inside_block, fixed_values
    )
    memory_state = memory_state * decay_per_block[:, None, None] + jnp.einsum(
        "wam,waz->wmz", damped_keys, fixed_values
    )
    return (memory_state, produced_rows)


def transition_step(carried, inputs):
    memory_state, transfer = carried
    state_updates, erase_term, inside_block, boosted_query, damped_keys, decay_per_block = inputs
    fixed_values = state_updates - jnp.einsum("mzq,mqc->mzc", erase_term, memory_state)
    coupling = jnp.einsum("hik,hil->hkl", damped_keys, erase_term)
    memory_state = memory_state * decay_per_block[:, None, None] + jnp.einsum(
        "wam,waz->wmz", damped_keys, fixed_values
    )
    transfer = transfer * decay_per_block[:, None, None] - jnp.einsum(
        "hkl,hlm->hkm", coupling, transfer
    )
    return ((memory_state, transfer), None)


def compose(prior_blocks, following_blocks):
    joined_map = jnp.einsum("hkl,hlm->hkm", following_blocks[0], prior_blocks[0])
    joined_state = (
        jnp.einsum("djo,dog->djg", following_blocks[0], prior_blocks[1]) + following_blocks[1]
    )
    return (joined_map, joined_state)


def stick_block(queries, key_rows, value_rows, query_place, key_place, offsets):
    scale_factor = queries.shape[-1] ** (-0.5)
    scores = (
        jnp.einsum("qhd,khd->hqk", queries, key_rows, preferred_element_type=jnp.float32)
        * scale_factor
        + offsets[:, None, None]
    )
    visible = key_place[None, :] < query_place[:, None]
    skipped = jnp.where(visible, jax.nn.log_sigmoid(-scores), 0.0)
    beyond = lax.cumsum(skipped, axis=2, reverse=True) - skipped
    weights = jnp.where(visible, jnp.exp(jax.nn.log_sigmoid(scores) + beyond), 0.0).astype(
        jnp.bfloat16
    )
    partial_value = jnp.einsum(
        "hqk,khd->qhd", weights, value_rows, preferred_element_type=jnp.float32
    )
    return (partial_value, jnp.sum(skipped, axis=2).T)


def stick_combine(partials, totals):
    beyond = jnp.cumsum(totals[::-1], axis=0)[::-1] - totals
    return jnp.sum(partials * jnp.exp(beyond)[..., None], axis=0)


def on_device(
    hidden_in,
    sb_query_w,
    sb_key_w,
    sb_value_w,
    sb_offset,
    delta_query_w,
    delta_key_w,
    delta_value_w,
    decay_w,
    write_w,
    write_bias,
    decay_log_scale,
    decay_shift,
    head_gain,
    sb_out_w,
    delta_out_w,
):
    token_rows = hidden_in.shape[1]
    local_in = hidden_in.reshape(token_rows, hidden_in.shape[2])
    gathered = (
        lax.all_gather(sb_query_w, "fs", axis=0, tiled=True),
        lax.all_gather(sb_key_w, "fs", axis=0, tiled=True),
        lax.all_gather(sb_value_w, "fs", axis=0, tiled=True),
        lax.all_gather(delta_query_w, "fs", axis=0, tiled=True),
        lax.all_gather(delta_key_w, "fs", axis=0, tiled=True),
        lax.all_gather(delta_value_w, "fs", axis=0, tiled=True),
    )
    in_weights = tuple(gathered) + (decay_w, write_w)
    portion = gathered_copies(local_in, "tp", 1)
    projected = tuple(
        (jnp.dot(portion, weight, preferred_element_type=jnp.float32) for weight in in_weights)
    )
    sb_heads = sb_offset.shape[0]
    delta_heads = decay_log_scale.shape[0]
    sb_query = projected[0].astype(jnp.bfloat16).reshape(token_rows, sb_heads, SB_DIM)
    sb_keys = projected[1].astype(jnp.bfloat16)
    sb_values = projected[2].astype(jnp.bfloat16)
    shift_rows = decay_shift.reshape(delta_heads, token_rows).T
    queries, key_rows, value_rows, log_decay, strength = delta_inputs(
        projected[3].astype(jnp.bfloat16),
        projected[4].astype(jnp.bfloat16),
        projected[5].astype(jnp.bfloat16),
        projected[6],
        projected[7],
        write_bias,
        decay_log_scale,
        shift_rows,
        delta_heads,
        GDN_DIM,
    )
    prepared = delta_prepare(
        to_blocks(queries, BLOCK),
        to_blocks(key_rows, BLOCK),
        to_blocks(value_rows, BLOCK),
        to_blocks(log_decay, BLOCK),
        to_blocks(strength, BLOCK),
    )
    identity_map = jnp.broadcast_to(
        jnp.eye(GDN_DIM, dtype=jnp.float32), (delta_heads, GDN_DIM, GDN_DIM)
    )
    empty_state = jnp.zeros((delta_heads, GDN_DIM, GDN_DIM), jnp.float32)
    (local_end, local_map), unused_out = lax.scan(
        transition_step, (empty_state, identity_map), prepared
    )
    own_first = lax.axis_index(SP) * token_rows
    query_place = own_first + lax.iota(jnp.int32, token_rows)
    sp_count = lax.axis_size(SP)
    slot_out = jnp.zeros((sp_count, token_rows, sb_heads, SB_DIM), jnp.float32)
    slot_total = jnp.zeros((sp_count, token_rows, sb_heads), jnp.float32)

    def absorb(slot_arrays, address_portion, value_part, shard_first):

        def active(current):
            partial_value, totals = stick_block(
                sb_query,
                address_portion.reshape(token_rows, sb_heads, SB_DIM),
                value_part.reshape(token_rows, sb_heads, SB_DIM),
                query_place,
                shard_first + lax.iota(jnp.int32, token_rows),
                sb_offset,
            )
            slot_index = shard_first // token_rows
            return (
                lax.dynamic_update_index_in_dim(current[0], partial_value, slot_index, 0),
                lax.dynamic_update_index_in_dim(current[1], totals, slot_index, 0),
            )

        def inactive(current):
            return current

        usable = jnp.logical_and(shard_first >= 0, shard_first <= own_first)
        return lax.cond(usable, active, inactive, slot_arrays)

    key_block, value_block = in_one_piece((sb_keys, sb_values), SP, 0, 1)

    def per_shard(shard_number, current):
        row_begin = shard_number * token_rows
        return absorb(
            current,
            lax.dynamic_slice_in_dim(key_block, row_begin, token_rows, 0),
            lax.dynamic_slice_in_dim(value_block, row_begin, token_rows, 0),
            row_begin,
        )

    slot_arrays = lax.fori_loop(
        0, key_block.shape[0] // token_rows, per_shard, (slot_out, slot_total)
    )
    unused_map, incoming = entering(
        (local_map, local_end), SP, compose, (identity_map, empty_state)
    )
    sb_mixed = (
        stick_combine(slot_arrays[0], slot_arrays[1])
        .astype(jnp.bfloat16)
        .reshape(token_rows, sb_heads * SB_DIM)
    )
    unused_end, produced_rows = lax.scan(delta_step, incoming, prepared)
    produced_rows = from_blocks(produced_rows)
    normed = (
        produced_rows
        * lax.rsqrt(jnp.mean(produced_rows * produced_rows, axis=-1, keepdims=True) + NORM_EPS)
        * head_gain
    )
    delta_mixed = normed.astype(jnp.bfloat16).reshape(token_rows, delta_heads * GDN_DIM)
    result = sent_and_summed(
        (
            jnp.dot(sb_mixed, sb_out_w, preferred_element_type=jnp.float32)
            + jnp.dot(delta_mixed, delta_out_w, preferred_element_type=jnp.float32)
        ).astype(jnp.bfloat16),
        "tp",
        0,
    )
    return result.astype(jnp.bfloat16).reshape(1, result.shape[0], result.shape[1])


def solution(mesh):
    finer = Mesh(
        mesh.devices.reshape(8, 4, mesh.shape["fs"], mesh.shape["tp"]), ("sp_0", "sp_1", "fs", "tp")
    )
    return jax.shard_map(
        on_device,
        mesh=finer,
        in_specs=(
            P("fs", SP, "tp"),
            P("fs", "tp"),
            P("fs", "tp"),
            P("fs", "tp"),
            P("tp"),
            P("fs", "tp"),
            P("fs", "tp"),
            P("fs", "tp"),
            P(None, "tp"),
            P(None, "tp"),
            P("tp"),
            P("tp"),
            P("fs", "tp", SP),
            P(),
            P("tp", None),
            P("tp", None),
        ),
        out_specs=P("fs", SP_TP, None),
        check_vma=False,
    )
```

profile of v0, /device:TPU:249, one launch (start us, length us, event | category | flops | bytes accessed | tf_op | source)
XLA Modules:
  0.0 923.9 jit_solution(8913548011204064963)
XLA Ops:
  22.8 19.7 %all-gather.22.cloned.1.call-done = bf16[2048,512]{1,0:T(8,128)(2,1)} async-done(((bf16[512,512]{1,0:T(8,128)(2,1)}), bf16[2048,512]{1,0:T(8,128)(2,1)}) %all-gather.22.cloned.1.call-update) | async-done | bytes 2097168 | tf_op jit(solution)/shard_map/all_gather | solution.py:233
  47.9 29.9 %all-gather.24.cloned.1.call-done = bf16[2048,512]{1,0:T(8,128)(2,1)} async-done(((bf16[512,512]{1,0:T(8,128)(2,1)}), bf16[2048,512]{1,0:T(8,128)(2,1)}) %all-gather.24.cloned.1.call-update) | async-done | bytes 2097168 | tf_op jit(solution)/shard_map/all_gather | solution.py:234
  133.6 14.4 %all-gather.14.cloned.1.call-done = bf16[2048,512]{1,0:T(8,128)(2,1)} async-done(((bf16[512,512]{1,0:T(8,128)(2,1)}), bf16[2048,512]{1,0:T(8,128)(2,1)}) %all-gather.14.cloned.1.call-update) | async-done | bytes 2097168 | tf_op jit(solution)/shard_map/all_gather | solution.py:230
  151.6 31.4 %all-gather.26.cloned.1.call-done = bf16[2048,512]{1,0:T(8,128)(2,1)} async-done(((bf16[512,512]{1,0:T(8,128)(2,1)}), bf16[2048,512]{1,0:T(8,128)(2,1)}) %all-gather.26.cloned.1.call-update) | async-done | bytes 2097168 | tf_op jit(solution)/shard_map/all_gather | solution.py:232
  187.3 30.9 %all-gather.20.cloned.1.call-done = bf16[2048,512]{1,0:T(8,128)(2,1)} async-done(((bf16[512,512]{1,0:T(8,128)(2,1)}), bf16[2048,512]{1,0:T(8,128)(2,1)}) %all-gather.20.cloned.1.call-update) | async-done | bytes 2097168 | tf_op jit(solution)/shard_map/all_gather | solution.py:229
  225.1 26.8 %all-gather.28.cloned.1.call-done = bf16[32,128,128]{2,1,0:T(8,128)(2,1)} async-done(((bf16[4,128,128]{2,1,0:T(8,128)(2,1)}), bf16[32,128,128]{2,1,0:T(8,128)(2,1)}) %all-gather.28.cloned.1.call-update) | async-done | bytes 1048592 | tf_op jit(solution)/shard_map/all_gather | solution.py:53
  252.0 38.6 %all-gather.30.cloned.1.call-done = bf16[32,128,128]{2,1,0:T(8,128)(2,1)} async-done(((bf16[4,128,128]{2,1,0:T(8,128)(2,1)}), bf16[32,128,128]{2,1,0:T(8,128)(2,1)}) %all-gather.30.cloned.1.call-update) | async-done | bytes 1048592 | tf_op jit(solution)/shard_map/all_gather | solution.py:53
  298.6 13.8 %while.42 = (s32[]{:T(128)}, f32[4,128,128]{2,1,0:T(8,128)S(1)}, f32[4,4,64,128]{3,2,1,0:T(8,128)S(1)}, f32[4,4]{1,0:T(4,128)S(1)}, bf16[4,4,64,128]{3,2,1,0:T(8...) while((s32[]{:T(128)}, f32[4,128,128]{2,1,0:T(8,128)S(1)}, ...), condition=%wide.region_15.16_spmd, body=%wide.region_14.15_spmd.sunk | while | flops 29589504 | bytes 2034329 | solution.py:324
  314.5 118.9 %all-gather.18.cloned.1.call-done = bf16[8192,1024]{1,0:T(8,128)(2,1)} async-done(((bf16[256,1024]{1,0:T(8,128)(2,1)}), bf16[8192,1024]{1,0:T(8,128)(2,1)}) %all-gather.18.cloned.1.call-update) | async-done | bytes 16777232 | tf_op jit(solution)/shard_map/all_gather | solution.py:37
  475.5 420.3 %while.44 = (s32[]{:T(128)}, f32[32,256,8,64]{1,3,2,0:T(8,128)}, f32[32,256,8]{1,2,0:T(8,128)S(1)}, s32[]{:T(128)}, bf16[8192,512]{0,1:T(8,128)(2,1)}, /*index=5...) while((s32[]{:T(128)}, f32[32,256,8,64]{1,3,2,0:T(8,128)}, ...), condition=%wide.region_6.7_spmd.clone.clone, body=%wide.region_0.6_spmd.clone.clone.sunk | while | flops 218698256 | bytes 25745960 | solution.py:313
  475.5 13.2 %conditional.4 = ((f32[32,256,8,64]{1,3,2,0:T(8,128)}, f32[32,256,8]{1,2,0:T(8,128)S(1)})) conditional(s32[]{:T(128)} %convert_element_type.285, (f32[32,256,8,64]{1,3,2,0:T(8,128)}, f32[32,256,8]{1,2,0:T(8,128)S(1)}) %tuple.97, (s32[]{:T(128)}, s32[]{:T(128)}, bf16[8192,512]{0,1:T(8,128)(2,1)}, bf16[256,8,64]{0,2,1:T(8,128)(2,1)S(1)}, ...), branch_computations={%region_1.1_spmd, %region_2.0_spmd} | conditional | flops 218698256 | bytes 25744700 | solution.py:300
  488.7 13.1 %conditional.4 = ((f32[32,256,8,64]{1,3,2,0:T(8,128)}, f32[32,256,8]{1,2,0:T(8,128)S(1)})) conditional(s32[]{:T(128)} %convert_element_type.285, (f32[32,256,8,64]{1,3,2,0:T(8,128)}, f32[32,256,8]{1,2,0:T(8,128)S(1)}) %tuple.97, (s32[]{:T(128)}, s32[]{:T(128)}, bf16[8192,512]{0,1:T(8,128)(2,1)}, bf16[256,8,64]{0,2,1:T(8,128)(2,1)S(1)}, ...), branch_computations={%region_1.1_spmd, %region_2.0_spmd} | conditional | flops 218698256 | bytes 25744700 | solution.py:300
  554.4 13.1 %conditional.4 = ((f32[32,256,8,64]{1,3,2,0:T(8,128)}, f32[32,256,8]{1,2,0:T(8,128)S(1)})) conditional(s32[]{:T(128)} %convert_element_type.285, (f32[32,256,8,64]{1,3,2,0:T(8,128)}, f32[32,256,8]{1,2,0:T(8,128)S(1)}) %tuple.97, (s32[]{:T(128)}, s32[]{:T(128)}, bf16[8192,512]{0,1:T(8,128)(2,1)}, bf16[256,8,64]{0,2,1:T(8,128)(2,1)S(1)}, ...), branch_computations={%region_1.1_spmd, %region_2.0_spmd} | conditional | flops 218698256 | bytes 25744700 | solution.py:300
  580.6 13.1 %conditional.4 = ((f32[32,256,8,64]{1,3,2,0:T(8,128)}, f32[32,256,8]{1,2,0:T(8,128)S(1)})) conditional(s32[]{:T(128)} %convert_element_type.285, (f32[32,256,8,64]{1,3,2,0:T(8,128)}, f32[32,256,8]{1,2,0:T(8,128)S(1)}) %tuple.97, (s32[]{:T(128)}, s32[]{:T(128)}, bf16[8192,512]{0,1:T(8,128)(2,1)}, bf16[256,8,64]{0,2,1:T(8,128)(2,1)S(1)}, ...), branch_computations={%region_1.1_spmd, %region_2.0_spmd} | conditional | flops 218698256 | bytes 25744700 | solution.py:300
  633.1 13.1 %conditional.4 = ((f32[32,256,8,64]{1,3,2,0:T(8,128)}, f32[32,256,8]{1,2,0:T(8,128)S(1)})) conditional(s32[]{:T(128)} %convert_element_type.285, (f32[32,256,8,64]{1,3,2,0:T(8,128)}, f32[32,256,8]{1,2,0:T(8,128)S(1)}) %tuple.97, (s32[]{:T(128)}, s32[]{:T(128)}, bf16[8192,512]{0,1:T(8,128)(2,1)}, bf16[256,8,64]{0,2,1:T(8,128)(2,1)S(1)}, ...), branch_computations={%region_1.1_spmd, %region_2.0_spmd} | conditional | flops 218698256 | bytes 25744700 | solution.py:300
  659.4 13.1 %conditional.4 = ((f32[32,256,8,64]{1,3,2,0:T(8,128)}, f32[32,256,8]{1,2,0:T(8,128)S(1)})) conditional(s32[]{:T(128)} %convert_element_type.285, (f32[32,256,8,64]{1,3,2,0:T(8,128)}, f32[32,256,8]{1,2,0:T(8,128)S(1)}) %tuple.97, (s32[]{:T(128)}, s32[]{:T(128)}, bf16[8192,512]{0,1:T(8,128)(2,1)}, bf16[256,8,64]{0,2,1:T(8,128)(2,1)S(1)}, ...), branch_computations={%region_1.1_spmd, %region_2.0_spmd} | conditional | flops 218698256 | bytes 25744700 | solution.py:300
  672.5 13.2 %conditional.4 = ((f32[32,256,8,64]{1,3,2,0:T(8,128)}, f32[32,256,8]{1,2,0:T(8,128)S(1)})) conditional(s32[]{:T(128)} %convert_element_type.285, (f32[32,256,8,64]{1,3,2,0:T(8,128)}, f32[32,256,8]{1,2,0:T(8,128)S(1)}) %tuple.97, (s32[]{:T(128)}, s32[]{:T(128)}, bf16[8192,512]{0,1:T(8,128)(2,1)}, bf16[256,8,64]{0,2,1:T(8,128)(2,1)S(1)}, ...), branch_computations={%region_1.1_spmd, %region_2.0_spmd} | conditional | flops 218698256 | bytes 25744700 | solution.py:300
  685.7 13.2 %conditional.4 = ((f32[32,256,8,64]{1,3,2,0:T(8,128)}, f32[32,256,8]{1,2,0:T(8,128)S(1)})) conditional(s32[]{:T(128)} %convert_element_type.285, (f32[32,256,8,64]{1,3,2,0:T(8,128)}, f32[32,256,8]{1,2,0:T(8,128)S(1)}) %tuple.97, (s32[]{:T(128)}, s32[]{:T(128)}, bf16[8192,512]{0,1:T(8,128)(2,1)}, bf16[256,8,64]{0,2,1:T(8,128)(2,1)S(1)}, ...), branch_computations={%region_1.1_spmd, %region_2.0_spmd} | conditional | flops 218698256 | bytes 25744700 | solution.py:300
  725.1 13.1 %conditional.4 = ((f32[32,256,8,64]{1,3,2,0:T(8,128)}, f32[32,256,8]{1,2,0:T(8,128)S(1)})) conditional(s32[]{:T(128)} %convert_element_type.285, (f32[32,256,8,64]{1,3,2,0:T(8,128)}, f32[32,256,8]{1,2,0:T(8,128)S(1)}) %tuple.97, (s32[]{:T(128)}, s32[]{:T(128)}, bf16[8192,512]{0,1:T(8,128)(2,1)}, bf16[256,8,64]{0,2,1:T(8,128)(2,1)S(1)}, ...), branch_computations={%region_1.1_spmd, %region_2.0_spmd} | conditional | flops 218698256 | bytes 25744700 | solution.py:300
  764.5 13.1 %conditional.4 = ((f32[32,256,8,64]{1,3,2,0:T(8,128)}, f32[32,256,8]{1,2,0:T(8,128)S(1)})) conditional(s32[]{:T(128)} %convert_element_type.285, (f32[32,256,8,64]{1,3,2,0:T(8,128)}, f32[32,256,8]{1,2,0:T(8,128)S(1)}) %tuple.97, (s32[]{:T(128)}, s32[]{:T(128)}, bf16[8192,512]{0,1:T(8,128)(2,1)}, bf16[256,8,64]{0,2,1:T(8,128)(2,1)S(1)}, ...), branch_computations={%region_1.1_spmd, %region_2.0_spmd} | conditional | flops 218698256 | bytes 25744700 | solution.py:300
  777.6 13.2 %conditional.4 = ((f32[32,256,8,64]{1,3,2,0:T(8,128)}, f32[32,256,8]{1,2,0:T(8,128)S(1)})) conditional(s32[]{:T(128)} %convert_element_type.285, (f32[32,256,8,64]{1,3,2,0:T(8,128)}, f32[32,256,8]{1,2,0:T(8,128)S(1)}) %tuple.97, (s32[]{:T(128)}, s32[]{:T(128)}, bf16[8192,512]{0,1:T(8,128)(2,1)}, bf16[256,8,64]{0,2,1:T(8,128)(2,1)S(1)}, ...), branch_computations={%region_1.1_spmd, %region_2.0_spmd} | conditional | flops 218698256 | bytes 25744700 | solution.py:300
  790.8 13.2 %conditional.4 = ((f32[32,256,8,64]{1,3,2,0:T(8,128)}, f32[32,256,8]{1,2,0:T(8,128)S(1)})) conditional(s32[]{:T(128)} %convert_element_type.285, (f32[32,256,8,64]{1,3,2,0:T(8,128)}, f32[32,256,8]{1,2,0:T(8,128)S(1)}) %tuple.97, (s32[]{:T(128)}, s32[]{:T(128)}, bf16[8192,512]{0,1:T(8,128)(2,1)}, bf16[256,8,64]{0,2,1:T(8,128)(2,1)S(1)}, ...), branch_computations={%region_1.1_spmd, %region_2.0_spmd} | conditional | flops 218698256 | bytes 25744700 | solution.py:300
  830.2 13.2 %conditional.4 = ((f32[32,256,8,64]{1,3,2,0:T(8,128)}, f32[32,256,8]{1,2,0:T(8,128)S(1)})) conditional(s32[]{:T(128)} %convert_element_type.285, (f32[32,256,8,64]{1,3,2,0:T(8,128)}, f32[32,256,8]{1,2,0:T(8,128)S(1)}) %tuple.97, (s32[]{:T(128)}, s32[]{:T(128)}, bf16[8192,512]{0,1:T(8,128)(2,1)}, bf16[256,8,64]{0,2,1:T(8,128)(2,1)S(1)}, ...), branch_computations={%region_1.1_spmd, %region_2.0_spmd} | conditional | flops 218698256 | bytes 25744700 | solution.py:300
  843.3 13.2 %conditional.4 = ((f32[32,256,8,64]{1,3,2,0:T(8,128)}, f32[32,256,8]{1,2,0:T(8,128)S(1)})) conditional(s32[]{:T(128)} %convert_element_type.285, (f32[32,256,8,64]{1,3,2,0:T(8,128)}, f32[32,256,8]{1,2,0:T(8,128)S(1)}) %tuple.97, (s32[]{:T(128)}, s32[]{:T(128)}, bf16[8192,512]{0,1:T(8,128)(2,1)}, bf16[256,8,64]{0,2,1:T(8,128)(2,1)S(1)}, ...), branch_computations={%region_1.1_spmd, %region_2.0_spmd} | conditional | flops 218698256 | bytes 25744700 | solution.py:300
  (637 shorter events, 843.2 us)
Async XLA Ops:
  6.5 901.7 %copy-start = (bf16[512,2048]{1,0:T(8,128)(2,1)S(1)}, bf16[512,2048]{1,0:T(8,128)(2,1)}, u32[]{:S(2)}) copy-start(bf16[512,2048]{1,0:T(8,128)(2,1)} %param.38) | copy-start | bytes 6291460
  6.5 3.4 copy-start.14
  6.5 35.9 %all-gather.22.cloned.1.call-start = ((), (), s32[]{:S(2)}) async-start(), calls=%async_computation.6 | async-start | bytes 2621440 | tf_op jit(solution)/shard_map/all_gather | solution.py:233
  7.3 70.5 %all-gather.24.cloned.1.call-start = ((), (), s32[]{:S(2)}) async-start(), calls=%async_computation.7 | async-start | bytes 2621440 | tf_op jit(solution)/shard_map/all_gather | solution.py:234
  8.0 123.0 %all-gather.16.cloned.1.call-start = ((), (), s32[]{:S(2)}) async-start(), calls=%async_computation.3 | async-start | bytes 2621440 | tf_op jit(solution)/shard_map/all_gather | solution.py:231
  8.7 139.3 %all-gather.14.cloned.1.call-start = ((), (), s32[]{:S(2)}) async-start(), calls=%async_computation.2 | async-start | bytes 2621440 | tf_op jit(solution)/shard_map/all_gather | solution.py:230
  9.3 173.8 %all-gather.26.cloned.1.call-start = ((), (), s32[]{:S(2)}) async-start(), calls=%async_computation.8 | async-start | bytes 2621440 | tf_op jit(solution)/shard_map/all_gather | solution.py:232
  10.1 7.1 copy-start.22
  10.1 8.2 copy-start.16
  10.2 8.2 copy-start.19
  11.3 9.9 %copy-start.17 = (bf16[2048,4]{0,1:T(4,128)(2,1)S(1)}, bf16[2048,4]{0,1:T(4,128)(2,1)}, u32[]{:S(2)}) copy-start(bf16[2048,4]{0,1:T(4,128)(2,1)} %param.33) | copy-start | bytes 49156
  11.3 9.9 %copy-start.20 = (f32[4]{0:T(128)S(1)}, f32[4]{0:T(128)}, u32[]{:S(2)}) copy-start(f32[4]{0:T(128)} %param.34) | copy-start | bytes 52
  11.3 7.1 all-to-all-start
  16.5 201.7 %all-gather.20.cloned.1.call-start = ((), (), s32[]{:S(2)}) async-start(), calls=%async_computation.5 | async-start | bytes 2621440 | tf_op jit(solution)/shard_map/all_gather | solution.py:229
  17.1 234.9 %all-gather.28.cloned.1.call-start = ((), (), s32[]{:S(2)}) async-start(), calls=%async_computation.9 | async-start | bytes 1179648 | tf_op jit(solution)/shard_map/all_gather | solution.py:53
  82.7 8.1 copy-start.2
  116.2 174.4 %all-gather.30.cloned.1.call-start = ((), (), s32[]{:S(2)}) async-start(), calls=%async_computation.10 | async-start | bytes 1179648 | tf_op jit(solution)/shard_map/all_gather | solution.py:53
  130.7 302.7 %all-gather.18.cloned.1.call-start = ((), (), s32[]{:S(2)}) async-start(), calls=%async_computation.4 | async-start | bytes 17301504 | tf_op jit(solution)/shard_map/all_gather | solution.py:37
  133.6 18.0 %copy-start.21 = (f32[128]{0:T(128)S(1)}, f32[128]{0:T(128)}, u32[]{:S(2)}) copy-start(f32[128]{0:T(128)} %param.37) | copy-start | bytes 1540
  220.8 3.1 copy-start.3
  252.0 42.2 %copy-start.1 = (bf16[32,128,128]{2,1,0:T(8,128)(2,1)S(1)}, bf16[32,128,128]{2,1,0:T(8,128)(2,1)}, u32[]{:S(2)}) copy-start(bf16[32,128,128]{2,1,0:T(8,128)(2,1)} %all-gather.28.cloned.1.call-done) | copy-start | bytes 3145732
  290.6 3.5 copy-start.13
  467.6 7.9 copy-start.15
  467.6 7.9 copy-start.18
  (9 other events, 11.5 us)
Sparse Core Ops, SparseCore 0:
  9.1 33.2 all-gather.21
  44.3 33.4 all-gather.23
  79.6 33.3 all-gather.15
  114.7 33.3 all-gather.13
  149.7 33.3 all-gather.25
  184.8 33.3 all-gather.19
  219.9 31.9 all-gather.27
  253.8 36.7 all-gather.29
  293.2 140.2 all-gather.17
where the time goes:
time: 927 us; the launch traced here: 924 us
  waiting for transfers between devices  316 us (34%)
  other arithmetic  287 us (31%)
  matrix products  160 us (17%)
  local copies, waits for them, and re-layouts  112 us (12%)
  blocking collectives  27.4 us (3%)
  between operations  13.9 us (1%)
    another operation x64, other arithmetic  164 us
    all_gather x1, waiting for transfers between devices, in_one_piece(): result = lax.all_gather(both, axis, axis=dim, tiled=True)  119 us
    convert_element_type x32, other arithmetic, stick_block(): jnp.where(visible, jnp.exp(jax.nn.log_sigmoid(scores) + beyond), 0.0)  97.4 us
    all_gather x2, waiting for transfers between devices, entering(): lax.all_gather(part.astype(kind), axis)  65.5 us
    dot_general x32, matrix products, stick_block(): jnp.einsum('qhd,khd->hqk', queries, key_rows, preferred_element_type=jnp....  56.7 us
    dot_general x32, matrix products, stick_block(): jnp.einsum('hqk,khd->qhd', weights, value_rows, preferred_element_type=jn...  35.6 us
    dynamic_slice x32, local copies, waits for them, and re-layouts, per_shard(): lax.dynamic_slice_in_dim(value_block, row_begin, token_rows, 0)  34.4 us
    all_gather x1, waiting for transfers between devices, on_device(): lax.all_gather(delta_query_w, 'fs', axis=0, tiled=True)  31.4 us
  transfers between devices with their start and end apart: 10, of which 9 were waited for; matrix products, arithmetic and copies ran while one was open for 9% of the time, Pallas kernels for 0%

commit v1 on v0

v1 whole, which is shorter than its diff:
```python
import functools

import jax
import jax.numpy as jnp
import numpy as np
from jax import lax
from jax.experimental import pallas as pl
from jax.experimental.pallas import tpu as pltpu
from jax.sharding import Mesh
from jax.sharding import PartitionSpec as P

f32 = jnp.float32
bf16 = jnp.bfloat16
LOG2E = float(np.log2(np.e))
EPS = 1e-6
CH = 256
NT = (((1,), (1,)), ((), ()))
Z = ("zh", "zl")
AXES = ("zh", "zl", "y", "fs", "tp")


def work_lists():
    place = lambda i, m, y: (m % 4) * 8 + (4 * i + y - m) // 4
    pairs = np.zeros((4, 2, 64), np.int32)
    single = np.zeros((4, 4, 8), np.int32)
    for y in range(4):
        steps = [(p, place(2 * p, m, y)) for p in (3, 2, 1, 0) for m in range(1, 8 * p + y + 1)]
        pairs[y, :, : len(steps)] = np.array(steps).T
        for chain, ps in enumerate(((3, 1), (2, 0))):
            steps = [(2 * p + 1, place(2 * p + 1, m, y)) for p in ps for m in range(1, 5)]
            single[y, 2 * chain : 2 * chain + 2] = np.array(steps).T
    return pairs, single


def stick_kernel(count_ref, pairs_ref, single_ref, off_ref, q_ref, kv_ref, u_ref, o_ref, acc, run, kt):
    off = off_ref[0]

    def turn(c, carry):
        kt[c] = jnp.transpose(kv_ref[c])
        return carry

    lax.fori_loop(0, 32, turn, 0, unroll=4)

    def tile(first_row, size, c, masked):
        rows = pl.ds(first_row, size)
        kv = kv_ref[c]
        z = jnp.dot(q_ref[rows, :], kt[c], preferred_element_type=f32) * (0.125 * LOG2E) + off
        sp = jnp.maximum(jnp.log2(1.0 + jnp.exp2(jnp.minimum(z, 40.0))), z)
        if masked:
            shape = (size, CH)
            seen = lax.broadcasted_iota(jnp.int32, shape, 1) < lax.broadcasted_iota(jnp.int32, shape, 0)
            sp = jnp.where(seen, sp, 0.0)
        after = jnp.dot(sp.astype(bf16), u_ref[...], preferred_element_type=f32)
        total = after[:, :1] + sp[:, :1]
        if masked:
            w = jnp.where(seen, jnp.exp2((z - sp) - after), 0.0)
            run[rows, :] = jnp.broadcast_to(total, (size, 128))
            acc[rows, :] = jnp.dot(w.astype(bf16), kv, preferred_element_type=f32)
        else:
            r = run[rows, :]
            w = jnp.exp2((z - sp) - (after + jnp.concatenate([r, r], axis=1)))
            run[rows, :] = r + total
            acc[rows, :] += jnp.dot(w.astype(bf16), kv, preferred_element_type=f32)

    def diagonal(n, carry):
        for k in range(2):
            tile(pl.multiple_of((2 * n + k) * CH, CH), CH, 2 * n + k, True)
        return carry

    lax.fori_loop(0, 4, diagonal, 0)

    def one(n, carry):
        for k in range(2):
            tile(pl.multiple_of(single_ref[2 * k, n] * CH, CH), CH, single_ref[2 * k + 1, n], False)
        return carry

    lax.fori_loop(0, 8, one, 0)

    def both(n, carry):
        tile(pl.multiple_of(pairs_ref[0, n] * 2 * CH, 2 * CH), 2 * CH, pairs_ref[1, n], False)
        return carry

    lax.fori_loop(0, count_ref[0], both, 0)
    lane = lax.broadcasted_iota(jnp.int32, (64, 128), 1)
    for d in range(16):
        low = acc[d * 128 : d * 128 + 64, :]
        high = acc[d * 128 + 64 : d * 128 + 128, :]
        o_ref[d] = jnp.where(lane < 64, pltpu.roll(low, 64, 1), high).astype(bf16)


def stick_attention(count, pairs, single, off, q, kv, u):
    smem = pl.BlockSpec(memory_space=pltpu.SMEM)
    vmem = pl.BlockSpec(memory_space=pltpu.VMEM)
    return pl.pallas_call(
        stick_kernel,
        out_shape=jax.ShapeDtypeStruct((16, 64, 128), bf16),
        in_specs=[smem] * 4 + [vmem] * 3,
        out_specs=vmem,
        scratch_shapes=[
            pltpu.VMEM((2048, 128), f32),
            pltpu.VMEM((2048, 128), f32),
            pltpu.VMEM((32, 128, CH), bf16),
        ],
        cost_estimate=pl.CostEstimate(flops=20_000_000_000, bytes_accessed=4_000_000, transcendentals=26_000_000),
        name="stick_attention",
    )(count, pairs, single, off, q, kv, u)


def mm(a, b, dims=(((1,), (0,)), ((), ()))):
    return lax.dot_general(a.astype(bf16), b.astype(bf16), dims, preferred_element_type=f32)


def silu(u):
    return u * jax.nn.sigmoid(u)


def unit(u):
    return u * lax.rsqrt(jnp.sum(u * u, axis=-1, keepdims=True) + EPS)


def delta_kernel(par_ref, proj_ref, shift_ref, qf_ref, of_ref, end_ref):
    minus_scale, bias = par_ref[0], par_ref[1]
    span = (CH, CH)
    row = lax.broadcasted_iota(jnp.int32, span, 0)
    col = lax.broadcasted_iota(jnp.int32, span, 1)
    same = (row // 64) == (col // 64)
    inclusive = jnp.logical_and(same, col <= row)
    strict = jnp.logical_and(same, col < row)
    sums = jnp.concatenate([jnp.where(inclusive, 1.0, 0.0), jnp.where(same, 1.0, 0.0)], axis=0)
    eye = jnp.where(row == col, 1.0, 0.0)
    lane = lax.broadcasted_iota(jnp.int32, (CH, 128), 1)
    tiles = range(4)
    cum, tot, q, k, v, beta = [], [], [], [], [], []
    for t in tiles:
        rows = slice(t * CH, (t + 1) * CH)
        proj = proj_ref[rows, :]
        dq, dk, dv = (proj[:, 128 * n : 128 * n + 128].astype(bf16).astype(f32) for n in range(3))
        pre = proj[:, 384:385]
        softplus = jnp.maximum(pre, 0.0) + jnp.log1p(jnp.exp(-jnp.abs(pre)))
        g = minus_scale * softplus + shift_ref[rows, :]
        beta.append(jax.nn.sigmoid(proj[:, 385:386] + bias))
        q.append(unit(silu(dq)) * 128**-0.5)
        k.append(unit(silu(dk)))
        v.append(silu(dv))
        g1 = g.astype(bf16).astype(f32)
        g2 = (g - g1).astype(bf16).astype(f32)
        g3 = g - g1 - g2
        parts = jnp.where(lane == 0, g1, jnp.where(lane == 1, g2, jnp.where(lane == 2, g3, 0.0)))
        s = mm(sums, parts)
        s = jnp.broadcast_to(s[:, 0:1] + s[:, 1:2] + s[:, 2:3], (2 * CH, 128))
        cum.append(s[:CH])
        tot.append(s[CH:])
    table = []
    for t in tiles:
        across = jnp.transpose(cum[t])[0:1, :]
        spread = cum[t][:, 0:1] - across
        table.append(jnp.where(inclusive, jnp.exp(jnp.where(inclusive, spread, 0.0)), 0.0))
    keys_beta = [k[t] * beta[t] for t in tiles]
    power = [jnp.where(strict, mm(keys_beta[t], k[t], NT) * table[t], 0.0) for t in tiles]
    inside = [mm(q[t], k[t], NT) * table[t] for t in tiles]
    inverse = [eye - power[t] for t in tiles]
    for _ in range(5):
        power = [mm(power[t], power[t]) for t in tiles]
        inverse = [inverse[t] + mm(inverse[t], power[t]) for t in tiles]
    growth = [jnp.exp(cum[t]) for t in tiles]
    both = [
        mm(inverse[t], jnp.concatenate([keys_beta[t] * growth[t], v[t] * beta[t]], axis=1)) for t in tiles
    ]
    seen = [mm(inside[t], both[t]) for t in tiles]
    reach = [q[t] * growth[t] - seen[t][:, :128] for t in tiles]
    own = [seen[t][:, 128:] for t in tiles]
    damped = [jnp.transpose(k[t] * jnp.exp(tot[t] - cum[t])) for t in tiles]
    wide = lax.broadcasted_iota(jnp.int32, (128, CH), 1) // 64
    small_eye = jnp.where(
        lax.broadcasted_iota(jnp.int32, (128, 128), 0) == lax.broadcasted_iota(jnp.int32, (128, 128), 1), 1.0, 0.0
    )
    maps = []
    for t in tiles:
        masked = jnp.concatenate([jnp.where(wide == b, damped[t], 0.0) for b in range(4)], axis=0)
        moved = mm(masked, both[t])
        for b in range(4):
            decay = jnp.exp(tot[t][b * 64 : b * 64 + 1, :])
            piece = moved[b * 128 : b * 128 + 128]
            maps.append((small_eye * decay - piece[:, :128], piece[:, 128:]))
    state = jnp.concatenate([small_eye, jnp.zeros((128, 128), f32)], axis=1)
    for n in range(16):
        t, b = n // 4, n % 4
        rows = slice(n * 64, n * 64 + 64)
        out = mm(reach[t][b * 64 : b * 64 + 64], state)
        qf_ref[rows, :] = out[:, :128]
        of_ref[rows, :] = out[:, 128:] + own[t][b * 64 : b * 64 + 64]
        state = mm(maps[n][0], state)
        state = jnp.concatenate([state[:, :128], state[:, 128:] + maps[n][1]], axis=1)
    end_ref[...] = state.astype(bf16)


def delta_local(par, proj, shift):
    vmem = pl.BlockSpec(memory_space=pltpu.VMEM)
    return pl.pallas_call(
        delta_kernel,
        out_shape=(
            jax.ShapeDtypeStruct((1024, 128), f32),
            jax.ShapeDtypeStruct((1024, 128), f32),
            jax.ShapeDtypeStruct((128, 256), bf16),
        ),
        in_specs=[pl.BlockSpec(memory_space=pltpu.SMEM), vmem, vmem],
        out_specs=(vmem, vmem, vmem),
        cost_estimate=pl.CostEstimate(flops=8_000_000_000, bytes_accessed=4_000_000, transcendentals=1_000_000),
        name="delta_local",
    )(par, proj, shift)


def finish_kernel(gain_ref, qf_ref, of_ref, *refs):
    maps, o_ref = refs[:-1], refs[-1]
    state = jnp.zeros((128, 128), f32)
    for ref in maps:
        state = mm(ref[:, :128], state) + ref[:, 128:].astype(f32)
    for t in range(4):
        rows = slice(t * CH, (t + 1) * CH)
        o = mm(qf_ref[rows, :], state) + of_ref[rows, :]
        o = o * lax.rsqrt(jnp.mean(o * o, axis=-1, keepdims=True) + EPS) * gain_ref[...]
        o_ref[rows, :] = o.astype(bf16)


def delta_finish(gain, qf, of, maps):
    vmem = pl.BlockSpec(memory_space=pltpu.VMEM)
    return pl.pallas_call(
        finish_kernel,
        out_shape=jax.ShapeDtypeStruct((1024, 128), bf16),
        in_specs=[vmem] * (3 + len(maps)),
        out_specs=vmem,
        cost_estimate=pl.CostEstimate(flops=1_000_000_000, bytes_accessed=2_000_000, transcendentals=2_000),
        name="delta_finish",
    )(gain, qf, of, *maps)


def ring(axis, size, step):
    return functools.partial(lax.ppermute, axis_name=axis, perm=[(i, (i + step) % size) for i in range(size)])


def placed(pieces, index, size, rows):
    whole = jnp.zeros((size * rows, *pieces[0].shape[1:]), pieces[0].dtype)
    for d, piece in enumerate(pieces):
        whole = lax.dynamic_update_slice_in_dim(whole, piece, ((index - d) % size) * rows, 0)
    return whole


def on_device(
    hidden_in,
    sb_query_w,
    sb_key_w,
    sb_value_w,
    sb_offset,
    delta_query_w,
    delta_key_w,
    delta_value_w,
    decay_w,
    write_w,
    write_bias,
    decay_log_scale,
    decay_shift,
    head_gain,
    sb_out_w,
    delta_out_w,
):
    z, y, fs, tp = lax.axis_index(Z), lax.axis_index("y"), lax.axis_index("fs"), lax.axis_index("tp")
    x = hidden_in.reshape(256, 1024)
    x_z = lax.all_gather(x, ("tp", *Z), axis=0, tiled=False).reshape(2, 2048, 1024)

    pick = lambda w, at, n: lax.dynamic_slice_in_dim(w, at, n, 1)
    mine = jnp.concatenate(
        [pick(sb_query_w, z * 64, 64), jnp.zeros((512, 64), bf16), pick(sb_key_w, z * 64, 64), pick(sb_value_w, z * 64, 64)]
        + [pick(w, y * 128, 128) for w in (delta_query_w, delta_key_w, delta_value_w)],
        axis=1,
    )
    weights = [mine] + [ring("fs", 4, d)(mine) for d in (1, 2, 3)]

    x_own = placed([x] + [ring("y", 4, d)(x) for d in (1, 2, 3)], y, 4, 256)
    swap = functools.partial(lax.ppermute, axis_name="tp", perm=[(0, 1), (1, 0)])
    x_other = swap(x_own)
    shift = decay_shift.reshape(4, 256)
    shifts = [shift] + [ring("y", 4, d)(shift) for d in (1, 2, 3)]
    shift_col = placed([pick(s.T, y, 1) for s in shifts], y, 4, 256)
    out_w = jnp.concatenate([sb_out_w, delta_out_w], axis=0)
    out_other = swap(out_w)

    w_all = placed(weights, fs, 4, 512)
    side = jnp.concatenate([pick(decay_w, y, 1), pick(write_w, y, 1), jnp.zeros((2048, 126), bf16)], axis=1)
    w_delta = jnp.concatenate([w_all[:, 256:], side], axis=1).reshape(2, 1024, 512)
    half = lambda w, at: lax.dynamic_index_in_dim(w, at, 0, keepdims=False)
    proj = jnp.dot(x_own, half(w_delta, tp), preferred_element_type=f32) + jnp.dot(
        x_other, half(w_delta, 1 - tp), preferred_element_type=f32
    )
    par = jnp.stack(
        [
            -jnp.exp(lax.dynamic_index_in_dim(decay_log_scale, y, 0, keepdims=False)),
            lax.dynamic_index_in_dim(write_bias, y, 0, keepdims=False),
        ]
    )
    qf, of, end = delta_local(par, proj, shift_col)
    ends = [lax.ppermute(end, Z, [(i, i + d) for i in range(8 - d)]) for d in range(7, 0, -1)]

    w_stick = w_all[:, :256]
    stick = (
        jnp.dot(x_z[0], w_stick[:1024], preferred_element_type=f32)
        + jnp.dot(x_z[1], w_stick[1024:], preferred_element_type=f32)
    ).astype(bf16)
    q, kv = stick[:, :128], stick[:, 128:]
    kv_all = jnp.concatenate([kv] + [ring("y", 4, d)(kv) for d in (1, 2, 3)], axis=0).reshape(32, CH, 128)
    pairs, single = work_lists()
    at_y = lambda table: lax.dynamic_index_in_dim(jnp.asarray(table), y, 0, keepdims=False)
    u = jnp.asarray(np.tril(np.ones((CH, CH), np.float32), -1), bf16)
    offset = lax.dynamic_slice_in_dim(sb_offset, z, 1, 0) * LOG2E
    count = (48 + 4 * y).astype(jnp.int32).reshape(1)
    sb = stick_attention(count, at_y(pairs), at_y(single), offset, q, kv_all, u)
    sb = lax.all_to_all(sb, (*Z, "tp"), 0, 0, tiled=True)

    dm = delta_finish(head_gain.reshape(1, 128), qf, of, ends)
    dm = lax.all_to_all(dm.reshape(8, 128, 128), ("y", "tp"), 0, 0, tiled=True)

    sb = sb.reshape(8, 2, 64, 2, 64).transpose(1, 3, 2, 0, 4).reshape(2, 128, 512)
    dm = dm.reshape(4, 2, 128, 128).transpose(1, 2, 0, 3).reshape(2, 128, 512)
    mixed = jnp.concatenate([sb, dm], axis=2)
    out = jnp.dot(half(mixed, tp), out_w, preferred_element_type=f32) + jnp.dot(
        half(mixed, 1 - tp), out_other, preferred_element_type=f32
    )
    return out.astype(bf16).reshape(1, 128, 2048)


def solution(mesh):
    finer = Mesh(mesh.devices.reshape(2, 4, 4, mesh.shape["fs"], mesh.shape["tp"]), AXES)
    sp = ("zh", "zl", "y")
    return jax.shard_map(
        on_device,
        mesh=finer,
        in_specs=(
            P("fs", sp, "tp"),
            P("fs", "tp"),
            P("fs", "tp"),
            P("fs", "tp"),
            P("tp"),
            P("fs", "tp"),
            P("fs", "tp"),
            P("fs", "tp"),
            P(None, "tp"),
            P(None, "tp"),
            P("tp"),
            P("tp"),
            P("fs", "tp", sp),
            P(),
            P("tp", None),
            P("tp", None),
        ),
        out_specs=P("fs", (*sp, "tp"), None),
        check_vma=False,
    )
```

time: 927 us -> 242 us (0.26)
  the two profiles are of different devices: /device:TPU:249 before, /device:TPU:25 now
where the time goes in v1:
time: 242 us; the launch traced here: 241 us
  starting transfers between devices  83 us (34%)
  Pallas kernels  59.9 us (25%)
  local copies, waits for them, and re-layouts  34.5 us (14%)
  waiting for transfers between devices  28.1 us (12%)
  matrix products  16.5 us (7%)
  between operations  15.2 us (6%)
  other arithmetic  3.42 us (1%)
    pallas_call x1, Pallas kernels, stick_attention(): pl.pallas_call(stick_kernel, out_shape=jax.ShapeDtypeStruct((16, 64, 128)...  45.9 us
    ppermute x7, starting transfers between devices, on_device(): lax.ppermute(end, Z, [(i, i + d) for i in range(8 - d)])  33.2 us
    ppermute x3, starting transfers between devices, on_device(): shifts = [shift] + [ring('y', 4, d)(shift) for d in (1, 2, 3)]  14.2 us
    all_to_all x1, starting transfers between devices, on_device(): sb = lax.all_to_all(sb, (*Z, 'tp'), 0, 0, tiled=True)  12 us
    all_to_all x1, waiting for transfers between devices, on_device(): sb = lax.all_to_all(sb, (*Z, 'tp'), 0, 0, tiled=True)  11.2 us
    pallas_call x1, Pallas kernels, delta_local(): pl.pallas_call(delta_kernel, out_shape=(jax.ShapeDtypeStruct((1024, 128),...  10.7 us
    dynamic_update_slice x12, local copies, waits for them, and re-layouts, placed(): lax.dynamic_update_slice_in_dim(whole, piece, (index - d) % size * rows, 0)  10.1 us
    all_to_all x1, starting transfers between devices, on_device(): dm = lax.all_to_all(dm.reshape(8, 128, 128), ('y', 'tp'), 0, 0, tiled=True)  9.14 us
  transfers between devices with their start and end apart: 24, of which 8 were waited for; matrix products, arithmetic and copies ran while one was open for 21% of the time, Pallas kernels for 25%

profile of v1, /device:TPU:25, one launch (start us, length us, event | category | flops | bytes accessed | tf_op | source)
XLA Modules:
  0.0 240.6 jit_solution(3327162114536333794)
XLA Ops:
  13.1 2.5 %collective-permute-start.1 = (bf16[512,640]{1,0:T(8,128)(2,1)}, bf16[512,640]{1,0:T(8,128)(2,1)}, u32[]{:S(2)}, u32[]{:S(2)}) collective-permute-start(bf16[512,640]{1,0:T(8,128)(2,1)} %concatenate.15), channel_id=1, source_target_pairs={{0,4},{2,6},{4,0},{6,2},{1,5},{3,7},{5,1},{7,3},{8,12},{10,14},{12... | collective-permute-start | bytes 1966088 | tf_op jit(solution)/shard_map/ppermute | solution.py:276
  15.5 2.2 collective-permute-start.7
  20.5 7.4 %collective-permute-done.6 = bf16[256,1024]{1,0:T(8,128)(2,1)S(1)} collective-permute-done((bf16[256,1024]{1,0:T(8,128)(2,1)S(1)}, bf16[256,1024]{1,0:T(8,128)(2,1)S(1)}, u32[]{:S(2)}, u32[]{:S(2)}) %collective-permute-start.6) | collective-permute-done | bytes 524320 | tf_op jit(solution)/shard_map/ppermute | solution.py:278
  29.9 11.6 %collective-permute-start.10 = (f32[4,256]{1,0:T(4,128)S(1)}, f32[4,256]{1,0:T(4,128)S(1)}, u32[]{:S(2)}, u32[]{:S(2)}) collective-permute-start(f32[4,256]{1,0:T(4,128)S(1)} %bitcast.65), channel_id=1, source_target_pairs={{0,8},{8,16},{16,24},{24,0},{1,9},{9,17},{17,25},{25,1},{2,10},{10... | collective-permute-start | bytes 12296 | tf_op jit(solution)/shard_map/ppermute | solution.py:282
  43.2 2.3 collective-permute-start.9
  48.9 3.2 %constant_dynamic-update-slice_fusion.13 = bf16[1024,2048]{1,0:T(8,128)(2,1)} fusion(bf16[512,2048]{1,0:T(8,128)(2,1)} %param.33), kind=kLoop, calls=%fused_computation.58 | loop fusion | bytes 4194304
  54.8 2.2 collective-permute-start.11
  57.0 1.9 collective-permute-done.11
  59.3 3.6 %collective-permute-done.12 = f32[4,256]{1,0:T(4,128)S(1)} collective-permute-done((f32[4,256]{1,0:T(4,128)S(1)}, f32[4,256]{1,0:T(4,128)S(1)}, u32[]{:S(2)}, u32[]{:S(2)}) %collective-permute-start.12) | collective-permute-done | bytes 4128 | tf_op jit(solution)/shard_map/ppermute | solution.py:282
  69.8 2.8 %fusion.4 = f32[1024,512]{1,0:T(8,128)S(1)} fusion(bf16[1024,1024]{1,0:T(8,128)(2,1)} %collective-permute-done.9, bf16[2,1024,512]{2,1,0:T(8,128)(2,1)S(1)} %bitcast.55, s32[]{:T(128)S(6)} %select_n.130), kind=kOutput, calls=%fused_computation.9 | convolution fusion | flops 1073741824 | bytes 5242884 | tf_op jit(solution)/shard_map/dot_general | solution.py:291
  72.7 4.2 %convolution_add_fusion.2.proj_ref = f32[1024,512]{1,0:T(8,128)} fusion(f32[1024,512]{1,0:T(8,128)S(1)} %fusion.4, bf16[1024,1024]{1,0:T(8,128)(2,1)} %constant_dynamic-update-slice_fusion.4, bf16[2,1024,512]{2,1,0:T(8,128)(2,1)S(1)} %bitcast.56, s32[]{:T(128)S(6)} %select_n.129), kind=kOutput, calls=%fused_computation.8 | convolution fusion | flops 1074266112 | bytes 7340036 | tf_op jit(solution)/shard_map/dot_general | solution.py:291
  76.8 10.7 %delta_local.1 = (f32[1024,128]{1,0:T(8,128)}, f32[1024,128]{1,0:T(8,128)}, bf16[128,256]{1,0:T(8,128)(2,1)}) custom-call(f32[2]{0:T(128)} %pad_maximum_fusion.1.par_ref, f32[1024,512]{1,0:T(8,128)} %convolution_add_fusion.2.proj_ref, f32[1024,1]{1,0:T(8,128)} %constant_dynamic-update-slice_fusion.shift_ref), custom_call_target="tpu_custom_call" | custom-call | flops 8000000000 | bytes 4000000 | tf_op jit(solution)/shard_map/delta_local/pallas_call | solution.py:199
  87.5 7.2 %collective-permute-start.13 = (bf16[128,256]{1,0:T(8,128)(2,1)}, bf16[128,256]{1,0:T(8,128)(2,1)S(1)}, u32[]{:S(2)}, u32[]{:S(2)}) collective-permute-start(bf16[128,256]{1,0:T(8,128)(2,1)} %get-tuple-element.10), channel_id=1, source_target_pairs={{0,224},{1,225},{2,226},{3,227},{4,228},{5,229},{6,230},{7,231},{8... | collective-permute-start | bytes 196616 | tf_op jit(solution)/shard_map/ppermute | solution.py:301
  96.3 4.0 %fusion.31 = (bf16[8,256,1024]{2,1,0:T(8,128)(2,1)S(1)}, bf16[8,256,1024]{2,1,0:T(8,128)(2,1)S(1)}) fusion(bf16[16,256,1024]{2,1,0:T(8,128)(2,1)} %all-gather.2.cloned.1.call-done), kind=kLoop, calls=%fused_computation.68 | loop fusion | bytes 16777216 | tf_op jit(solution)/shard_map/slice | solution.py:305
  107.4 3.1 %collective-permute-start.20 = (bf16[1024,2048]{1,0:T(8,128)(2,1)}, bf16[1024,2048]{1,0:T(8,128)(2,1)}, u32[]{:S(2)}, u32[]{:S(2)}) collective-permute-start(bf16[1024,2048]{1,0:T(8,128)(2,1)} %constant_dynamic-update-slice_fusion.12), channel_id=1, source_target_pairs={{0,1},{1,0},{2,3},{3,2},{4,5},{5,4},{6,7},{7,6},{8,9},{9,8},{10,11... | collective-permute-start | bytes 12582920 | tf_op jit(solution)/shard_map/ppermute | solution.py:285
  116.0 10.2 %collective-permute-start.17 = (bf16[128,256]{1,0:T(8,128)(2,1)S(1)}, bf16[128,256]{1,0:T(8,128)(2,1)S(1)}, u32[]{:S(2)}, u32[]{:S(2)}) collective-permute-start(bf16[128,256]{1,0:T(8,128)(2,1)S(1)} %copy-done.9), channel_id=1, source_target_pairs={{0,96},{32,128},{64,160},{96,192},{128,224},{1,97},{33,129},{65,16... | collective-permute-start | bytes 196616 | tf_op jit(solution)/shard_map/ppermute | solution.py:301
  127.6 10.5 %collective-permute-start.18 = (bf16[128,256]{1,0:T(8,128)(2,1)S(1)}, bf16[128,256]{1,0:T(8,128)(2,1)S(1)}, u32[]{:S(2)}, u32[]{:S(2)}) collective-permute-start(bf16[128,256]{1,0:T(8,128)(2,1)S(1)} %copy-done.9), channel_id=1, source_target_pairs={{0,64},{32,96},{64,128},{96,160},{128,192},{160,224},{1,65},{33,97... | collective-permute-start | bytes 196616 | tf_op jit(solution)/shard_map/ppermute | solution.py:301
  142.6 3.3 %delta_finish.1 = bf16[1024,128]{1,0:T(8,128)(2,1)} custom-call(f32[1,128]{1,0:T(1,128)} %bitcast.68, f32[1024,128]{1,0:T(8,128)} %get-tuple-element.8.qf_ref, f32[1024,128]{1,0:T(8,128)} %get-tuple-element.9.of_ref, bf16[128,256]{1,0:T(8,128)(2,1)} %copy-done.10, bf16[128,256]{1,0:T(8,128)(2,1)} %copy-done.11, bf16[128,256]{1,0:T(8,128)(2,1)} %copy-done.12, ...), custom_call_target="tpu_custom_call" | custom-call | flops 1000000000 | bytes 2000000 | tf_op jit(solution)/shard_map/delta_finish/pallas_call | solution.py:227
  145.9 9.1 %all-to-all-start.1 = ((bf16[8,128,128]{2,1,0:T(8,128)(2,1)}), bf16[8,128,128]{2,1,0:T(8,128)(2,1)S(1)}, u32[]{:S(2)}, u32[]{:S(2)}) async-start(bf16[8,128,128]{2,1,0:T(8,128)(2,1)} %bitcast.64), calls=%async_computation.1 | async-start | bytes 524288 | tf_op jit(solution)/shard_map/all_to_all | solution.py:319
  156.6 45.9 %stick_attention.1 = bf16[16,64,128]{2,1,0:T(8,128)(2,1)} custom-call(s32[1]{0:T(128)} %bitcast.count_ref, s32[2,64]{1,0:T(2,128)} %fusion.24.pairs_ref, s32[4,8]{1,0:T(4,128)} %fusion.23.single_ref, f32[1]{0:T(128)S(6)} %mul.49.off_ref, bf16[2048,128]{1,0:T(8,128)(2,1)} %get-tuple-element.14.q_ref, bf16[32,256,128]{2,1,0:T(8,128)(2,1)} %bitcast.57, ...), custom_call_target="tpu_custom_call" | custom-call | flops 20000000000 | bytes 4000000 | tf_op jit(solution)/shard_map/stick_attention/pallas_call | solution.py:94
  202.5 12.0 %all-to-all-start = ((bf16[16,64,128]{2,1,0:T(8,128)(2,1)}), bf16[16,64,128]{2,1,0:T(8,128)(2,1)S(1)}, u32[]{:S(2)}, u32[]{:S(2)}) async-start(bf16[16,64,128]{2,1,0:T(8,128)(2,1)} %stick_attention.1), calls=%async_computation | async-start | bytes 524288 | tf_op jit(solution)/shard_map/all_to_all | solution.py:316
  214.8 11.2 %all-to-all-done = bf16[16,64,128]{2,1,0:T(8,128)(2,1)S(1)} async-done(((bf16[16,64,128]{2,1,0:T(8,128)(2,1)}), bf16[16,64,128]{2,1,0:T(8,128)(2,1)S(1)}, u32[]{:S(2)}, u32[]{:S(2)}) %all-to-all-start) | async-done | bytes 262176 | tf_op jit(solution)/shard_map/all_to_all | solution.py:316
  227.0 3.0 %fusion.17 = f32[128,2048]{1,0:T(8,128)S(1)} fusion(bf16[1024,2048]{1,0:T(8,128)(2,1)} %constant_dynamic-update-slice_fusion.12, s32[]{:T(128)S(6)} %select_n.129, bf16[2,128,512]{2,1,0:T(8,128)(2,1)S(1)} %reshape.53, bf16[2,128,512]{2,1,0:T(8,128)(2,1)S(1)} %copy.55), kind=kOutput, calls=%fused_computation.26 | convolution fusion | flops 537395200 | bytes 5767172 | tf_op jit(solution)/shard_map/dot_general | solution.py:324
  230.0 3.8 %fusion.3 = bf16[1,128,2048]{2,1,0:T(8,128)(2,1)} fusion(f32[128,2048]{1,0:T(8,128)S(1)} %fusion.17, bf16[1024,2048]{1,0:T(8,128)(2,1)} %collective-permute-done.20, s32[]{:T(128)S(6)} %select_n.130, bf16[2,128,512]{2,1,0:T(8,128)(2,1)S(1)} %reshape.53, bf16[2,128,512]{2,1,0:T(8,128)(2,1)S(1)} %copy.55), kind=kOutput, calls=%fused_computation.5 | convolution fusion | flops 537919488 | bytes 6291460 | tf_op jit(solution)/shard_map/dot_general | solution.py:324
  (126 shorter events, 47.6 us)
Async XLA Ops:
  6.5 89.7 %all-gather.2.cloned.1.call-start = ((), (), s32[]{:S(2)}) async-start(), calls=%async_computation.2 | async-start | bytes 8912896 | tf_op jit(solution)/shard_map/all_gather | solution.py:268
  11.9 53.5 %collective-permute-start = (bf16[512,640]{1,0:T(8,128)(2,1)}, bf16[512,640]{1,0:T(8,128)(2,1)}, u32[]{:S(2)}, u32[]{:S(2)}) collective-permute-start(bf16[512,640]{1,0:T(8,128)(2,1)} %concatenate.15), channel_id=1, source_target_pairs={{0,2},{2,4},{4,6},{6,0},{1,3},{3,5},{5,7},{7,1},{8,10},{10,12},{12... | collective-permute-start | bytes 1966088 | tf_op jit(solution)/shard_map/ppermute | solution.py:276
  13.1 53.5 %collective-permute-start.1 = (bf16[512,640]{1,0:T(8,128)(2,1)}, bf16[512,640]{1,0:T(8,128)(2,1)}, u32[]{:S(2)}, u32[]{:S(2)}) collective-permute-start(bf16[512,640]{1,0:T(8,128)(2,1)} %concatenate.15), channel_id=1, source_target_pairs={{0,4},{2,6},{4,0},{6,2},{1,5},{3,7},{5,1},{7,3},{8,12},{10,14},{12... | collective-permute-start | bytes 1966088 | tf_op jit(solution)/shard_map/ppermute | solution.py:276
  15.5 12.3 %collective-permute-start.6 = (bf16[256,1024]{1,0:T(8,128)(2,1)S(1)}, bf16[256,1024]{1,0:T(8,128)(2,1)S(1)}, u32[]{:S(2)}, u32[]{:S(2)}) collective-permute-start(bf16[256,1024]{1,0:T(8,128)(2,1)S(1)} %bitcast.58), channel_id=1, source_target_pairs={{0,8},{8,16},{16,24},{24,0},{1,9},{9,17},{17,25},{25,1},{2,10},{10... | collective-permute-start | bytes 1572872 | tf_op jit(solution)/shard_map/ppermute | solution.py:278
  15.5 14.3 %collective-permute-start.7 = (bf16[256,1024]{1,0:T(8,128)(2,1)S(1)}, bf16[256,1024]{1,0:T(8,128)(2,1)S(1)}, u32[]{:S(2)}, u32[]{:S(2)}) collective-permute-start(bf16[256,1024]{1,0:T(8,128)(2,1)S(1)} %bitcast.59), channel_id=1, source_target_pairs={{0,16},{8,24},{16,0},{24,8},{1,17},{9,25},{17,1},{25,9},{2,18},{10... | collective-permute-start | bytes 1572872 | tf_op jit(solution)/shard_map/ppermute | solution.py:278
  17.8 24.6 %collective-permute-start.8 = (bf16[256,1024]{1,0:T(8,128)(2,1)S(1)}, bf16[256,1024]{1,0:T(8,128)(2,1)S(1)}, u32[]{:S(2)}, u32[]{:S(2)}) collective-permute-start(bf16[256,1024]{1,0:T(8,128)(2,1)S(1)} %bitcast.60), channel_id=1, source_target_pairs={{0,24},{8,0},{16,8},{24,16},{1,25},{9,1},{17,9},{25,17},{2,26},{10... | collective-permute-start | bytes 1572872 | tf_op jit(solution)/shard_map/ppermute | solution.py:278
  27.9 39.9 %collective-permute-start.2 = (bf16[512,640]{1,0:T(8,128)(2,1)}, bf16[512,640]{1,0:T(8,128)(2,1)}, u32[]{:S(2)}, u32[]{:S(2)}) collective-permute-start(bf16[512,640]{1,0:T(8,128)(2,1)} %concatenate.15), channel_id=1, source_target_pairs={{0,6},{2,0},{4,2},{6,4},{1,7},{3,1},{5,3},{7,5},{8,14},{10,8},{12,... | collective-permute-start | bytes 1966088 | tf_op jit(solution)/shard_map/ppermute | solution.py:276
  29.9 24.9 %collective-permute-start.10 = (f32[4,256]{1,0:T(4,128)S(1)}, f32[4,256]{1,0:T(4,128)S(1)}, u32[]{:S(2)}, u32[]{:S(2)}) collective-permute-start(f32[4,256]{1,0:T(4,128)S(1)} %bitcast.65), channel_id=1, source_target_pairs={{0,8},{8,16},{16,24},{24,0},{1,9},{9,17},{17,25},{25,1},{2,10},{10... | collective-permute-start | bytes 12296 | tf_op jit(solution)/shard_map/ppermute | solution.py:282
  43.2 26.6 %collective-permute-start.9 = (bf16[1024,1024]{1,0:T(8,128)(2,1)}, bf16[1024,1024]{1,0:T(8,128)(2,1)}, u32[]{:S(2)}, u32[]{:S(2)}) collective-permute-start(bf16[1024,1024]{1,0:T(8,128)(2,1)} %constant_dynamic-update-slice_fusion.4), channel_id=1, source_target_pairs={{0,1},{1,0},{2,3},{3,2},{4,5},{5,4},{6,7},{7,6},{8,9},{9,8},{10,11... | collective-permute-start | bytes 6291464 | tf_op jit(solution)/shard_map/ppermute | solution.py:280
  54.8 4.0 %collective-permute-start.11 = (f32[4,256]{1,0:T(4,128)S(1)}, f32[4,256]{1,0:T(4,128)S(1)}, u32[]{:S(2)}, u32[]{:S(2)}) collective-permute-start(f32[4,256]{1,0:T(4,128)S(1)} %bitcast.66), channel_id=1, source_target_pairs={{0,16},{8,24},{16,0},{24,8},{1,17},{9,25},{17,1},{25,9},{2,18},{10... | collective-permute-start | bytes 12296 | tf_op jit(solution)/shard_map/ppermute | solution.py:282
  58.9 4.1 %collective-permute-start.12 = (f32[4,256]{1,0:T(4,128)S(1)}, f32[4,256]{1,0:T(4,128)S(1)}, u32[]{:S(2)}, u32[]{:S(2)}) collective-permute-start(f32[4,256]{1,0:T(4,128)S(1)} %bitcast.67), channel_id=1, source_target_pairs={{0,24},{8,0},{16,8},{24,16},{1,25},{9,1},{17,9},{25,17},{2,26},{10... | collective-permute-start | bytes 12296 | tf_op jit(solution)/shard_map/ppermute | solution.py:282
  87.5 19.9 %collective-permute-start.13 = (bf16[128,256]{1,0:T(8,128)(2,1)}, bf16[128,256]{1,0:T(8,128)(2,1)S(1)}, u32[]{:S(2)}, u32[]{:S(2)}) collective-permute-start(bf16[128,256]{1,0:T(8,128)(2,1)} %get-tuple-element.10), channel_id=1, source_target_pairs={{0,224},{1,225},{2,226},{3,227},{4,228},{5,229},{6,230},{7,231},{8... | collective-permute-start | bytes 196616 | tf_op jit(solution)/shard_map/ppermute | solution.py:301
  94.7 15.8 %collective-permute-start.14 = (bf16[128,256]{1,0:T(8,128)(2,1)}, bf16[128,256]{1,0:T(8,128)(2,1)S(1)}, u32[]{:S(2)}, u32[]{:S(2)}) collective-permute-start(bf16[128,256]{1,0:T(8,128)(2,1)} %get-tuple-element.10), channel_id=1, source_target_pairs={{0,192},{32,224},{1,193},{33,225},{2,194},{34,226},{3,195},{35,227... | collective-permute-start | bytes 196616 | tf_op jit(solution)/shard_map/ppermute | solution.py:301
  103.9 51.2 %collective-permute-start.3 = (bf16[2048,128]{1,0:T(8,128)(2,1)S(1)}, bf16[2048,128]{1,0:T(8,128)(2,1)S(1)}, u32[]{:S(2)}, u32[]{:S(2)}) collective-permute-start(bf16[2048,128]{1,0:T(8,128)(2,1)S(1)} %get-tuple-element.13), channel_id=1, source_target_pairs={{0,8},{8,16},{16,24},{24,0},{1,9},{9,17},{17,25},{25,1},{2,10},{10... | collective-permute-start | bytes 1572872 | tf_op jit(solution)/shard_map/ppermute | solution.py:309
  103.9 51.2 %collective-permute-start.4 = (bf16[2048,128]{1,0:T(8,128)(2,1)S(1)}, bf16[2048,128]{1,0:T(8,128)(2,1)S(1)}, u32[]{:S(2)}, u32[]{:S(2)}) collective-permute-start(bf16[2048,128]{1,0:T(8,128)(2,1)S(1)} %get-tuple-element.13), channel_id=1, source_target_pairs={{0,16},{8,24},{16,0},{24,8},{1,17},{9,25},{17,1},{25,9},{2,18},{10... | collective-permute-start | bytes 1572872 | tf_op jit(solution)/shard_map/ppermute | solution.py:309
  105.1 49.9 %collective-permute-start.5 = (bf16[2048,128]{1,0:T(8,128)(2,1)S(1)}, bf16[2048,128]{1,0:T(8,128)(2,1)S(1)}, u32[]{:S(2)}, u32[]{:S(2)}) collective-permute-start(bf16[2048,128]{1,0:T(8,128)(2,1)S(1)} %get-tuple-element.13), channel_id=1, source_target_pairs={{0,24},{8,0},{16,8},{24,16},{1,25},{9,1},{17,9},{25,17},{2,26},{10... | collective-permute-start | bytes 1572872 | tf_op jit(solution)/shard_map/ppermute | solution.py:309
  107.4 122.5 %collective-permute-start.20 = (bf16[1024,2048]{1,0:T(8,128)(2,1)}, bf16[1024,2048]{1,0:T(8,128)(2,1)}, u32[]{:S(2)}, u32[]{:S(2)}) collective-permute-start(bf16[1024,2048]{1,0:T(8,128)(2,1)} %constant_dynamic-update-slice_fusion.12), channel_id=1, source_target_pairs={{0,1},{1,0},{2,3},{3,2},{4,5},{5,4},{6,7},{7,6},{8,9},{9,8},{10,11... | collective-permute-start | bytes 12582920 | tf_op jit(solution)/shard_map/ppermute | solution.py:285
  110.5 2.9 %collective-permute-start.15 = (bf16[128,256]{1,0:T(8,128)(2,1)S(1)}, bf16[128,256]{1,0:T(8,128)(2,1)S(1)}, u32[]{:S(2)}, u32[]{:S(2)}) collective-permute-start(bf16[128,256]{1,0:T(8,128)(2,1)S(1)} %copy-done.9), channel_id=1, source_target_pairs={{0,160},{32,192},{64,224},{1,161},{33,193},{65,225},{2,162},{34,19... | collective-permute-start | bytes 196616 | tf_op jit(solution)/shard_map/ppermute | solution.py:301
  113.4 2.6 %collective-permute-start.16 = (bf16[128,256]{1,0:T(8,128)(2,1)S(1)}, bf16[128,256]{1,0:T(8,128)(2,1)S(1)}, u32[]{:S(2)}, u32[]{:S(2)}) collective-permute-start(bf16[128,256]{1,0:T(8,128)(2,1)S(1)} %copy-done.9), channel_id=1, source_target_pairs={{0,128},{32,160},{64,192},{96,224},{1,129},{33,161},{65,193},{97,2... | collective-permute-start | bytes 196616 | tf_op jit(solution)/shard_map/ppermute | solution.py:301
  116.0 11.5 %collective-permute-start.17 = (bf16[128,256]{1,0:T(8,128)(2,1)S(1)}, bf16[128,256]{1,0:T(8,128)(2,1)S(1)}, u32[]{:S(2)}, u32[]{:S(2)}) collective-permute-start(bf16[128,256]{1,0:T(8,128)(2,1)S(1)} %copy-done.9), channel_id=1, source_target_pairs={{0,96},{32,128},{64,160},{96,192},{128,224},{1,97},{33,129},{65,16... | collective-permute-start | bytes 196616 | tf_op jit(solution)/shard_map/ppermute | solution.py:301
  127.6 11.8 %collective-permute-start.18 = (bf16[128,256]{1,0:T(8,128)(2,1)S(1)}, bf16[128,256]{1,0:T(8,128)(2,1)S(1)}, u32[]{:S(2)}, u32[]{:S(2)}) collective-permute-start(bf16[128,256]{1,0:T(8,128)(2,1)S(1)} %copy-done.9), channel_id=1, source_target_pairs={{0,64},{32,96},{64,128},{96,160},{128,192},{160,224},{1,65},{33,97... | collective-permute-start | bytes 196616 | tf_op jit(solution)/shard_map/ppermute | solution.py:301
  139.3 2.7 %collective-permute-start.19 = (bf16[128,256]{1,0:T(8,128)(2,1)S(1)}, bf16[128,256]{1,0:T(8,128)(2,1)S(1)}, u32[]{:S(2)}, u32[]{:S(2)}) collective-permute-start(bf16[128,256]{1,0:T(8,128)(2,1)S(1)} %copy-done.9), channel_id=1, source_target_pairs={{0,32},{32,64},{64,96},{96,128},{128,160},{160,192},{192,224},{1,3... | collective-permute-start | bytes 196616 | tf_op jit(solution)/shard_map/ppermute | solution.py:301
  145.9 56.6 %all-to-all-start.1 = ((bf16[8,128,128]{2,1,0:T(8,128)(2,1)}), bf16[8,128,128]{2,1,0:T(8,128)(2,1)S(1)}, u32[]{:S(2)}, u32[]{:S(2)}) async-start(bf16[8,128,128]{2,1,0:T(8,128)(2,1)} %bitcast.64), calls=%async_computation.1 | async-start | bytes 524288 | tf_op jit(solution)/shard_map/all_to_all | solution.py:319
  202.5 23.5 %all-to-all-start = ((bf16[16,64,128]{2,1,0:T(8,128)(2,1)}), bf16[16,64,128]{2,1,0:T(8,128)(2,1)S(1)}, u32[]{:S(2)}, u32[]{:S(2)}) async-start(bf16[16,64,128]{2,1,0:T(8,128)(2,1)} %stick_attention.1), calls=%async_computation | async-start | bytes 524288 | tf_op jit(solution)/shard_map/all_to_all | solution.py:316
  (20 other events, 283.3 us)
Sparse Core Ops, SparseCore 0:
  9.2 58.9 all-gather.1
